TPU v7x, 32 devices: a whole 2x2x4 slice. The times are simulated.
32 devices in a mesh: sp: 8 (over z, core), tp: 4 (over y, x).
Axes of the slice: x: 2, y: 2, z: 4, core: 2. Of those that a mesh axis runs over, the one named last changes fastest.
Arguments:
- residual_in: bfloat16 [2048, 2048], P(('sp', 'tp')), may hold values from -6 to 6
- query_a: bfloat16 [2048, 1024], P('sp', 'tp'), may hold values from -12 to 12
- key_a: bfloat16 [2048, 1024], P('sp', 'tp'), may hold values from -12 to 12
- value_a: bfloat16 [2048, 1024], P('sp', 'tp'), may hold values from -6 to 6
- query_b: bfloat16 [2048, 2048], P('sp', 'tp'), may hold values from -12 to 12
- key_b: bfloat16 [2048, 2048], P('sp', 'tp'), may hold values from -12 to 12
- value_b: bfloat16 [2048, 2048], P('sp', 'tp'), may hold values from -6 to 6
- cum_gates: float32 [2048, 2, 16], P('sp', None, 'tp'), may hold values from -247.76 to 0, as said below
- out_a: bfloat16 [1024, 2048], P('tp'), may hold values from -0.1875 to 0.1875
- out_b: bfloat16 [2048, 2048], P('tp'), may hold values from -0.125 to 0.125
- post_gain: bfloat16 [2048], replicated, may hold values from 0.099609375 to 1.8984375
- pre_gain: bfloat16 [2048], replicated, may hold values from 0.099609375 to 1.8984375
- expert_ids: int32 [2048, 2], P('sp'), may hold values from 0 to 7, all different within a row; in each aligned block of 256 rows (0 to 255, 256 to 511, ...) at most 80 rows name the same one
- expert_weights: float32 [2048, 2], P('sp'), may hold values from 0.2 to 1
- w_gate: bfloat16 [8, 2048, 4096], P('sp', None, 'tp'), may hold values from -0.125 to 0.125
- w_up: bfloat16 [8, 2048, 4096], P('sp', None, 'tp'), may hold values from -0.125 to 0.125
- w_down: bfloat16 [8, 4096, 2048], P('sp', 'tp'), may hold values from -0.09375 to 0.09375
Outputs:
- layer_out: bfloat16 [2048, 2048], P(('sp', 'tp'))
Inputs may be any that keep to these rules, and one draw needn't show every extreme that they name: `expert_ids`: in each aligned block of 256 positions no expert is named by more than 80 routes, a bound that some block reaches; a token's experts differ. `cum_gates`: never rises along the positions.
All inputs are finite; a program needn't handle non-finite values.
Results may differ from a plain program's by a relative error of at most 0.015.
Values may be sent and summed in bfloat16 or wider, within the bound.
A program may use at most 64 MiB of HBM per device.

v0:
```python
import jax
import jax.numpy as jnp
from jax import lax
from jax.sharding import PartitionSpec as P

eps_norm = 1e-06
big_neg = -1e30


def rms_scale(values, gain):
    return values * lax.rsqrt(jnp.mean(values * values, axis=-1, keepdims=True) + eps_norm) * gain


def empty_state(item_count, heads, width):
    return (
        jnp.full((heads, item_count), big_neg, jnp.float32),
        jnp.zeros((heads, item_count), jnp.float32),
        jnp.zeros((heads, item_count, width), jnp.float32),
    )


def update_state(state, query, key_rows, values, query_gate, key_gate, mask, width):
    highest, total, accum = state
    score = jnp.einsum(
        "rhd,khd->hrk", query, key_rows, preferred_element_type=jnp.float32
    ) * width ** (-0.5)
    score = score + query_gate.T[:, :, None] - key_gate.T[:, None, :]
    new_high = jnp.maximum(highest, jnp.max(jnp.where(mask[None], score, big_neg), axis=2))
    expo = jnp.exp(jnp.where(mask[None], score - new_high[:, :, None], big_neg))
    total = jnp.sum(expo, axis=2)
    accum = jnp.einsum(
        "hrk,khd->hrd", expo.astype(jnp.bfloat16), values, preferred_element_type=jnp.float32
    )
    return (new_high, total, accum)


def finish(state):
    highest, total, accum = state
    heads, item_count, width = accum.shape
    result = accum / total[:, :, None]
    return result.transpose(1, 0, 2).reshape(item_count, heads * width).astype(jnp.bfloat16)


def per_device(
    residual_in,
    query_a,
    key_a,
    value_a,
    query_b,
    key_b,
    value_b,
    cum_gates,
    out_a,
    out_b,
    post_gain,
    pre_gain,
    expert_ids,
    expert_weights,
    w_gate,
    w_up,
    w_down,
):
    rows = query_a.shape[0]
    heads = cum_gates.shape[2]
    width_a = query_a.shape[1] // heads
    width_b = query_b.shape[1] // heads
    group_size = lax.axis_size("sp")
    narrow = lax.axis_size("tp")
    here = lax.axis_index("sp")
    offset = here * rows
    gates_all = lax.all_gather(cum_gates, "sp", axis=0, tiled=True)
    queries_a = query_a.reshape(rows, heads, width_a)
    queries_b = query_b.reshape(rows, heads, width_b)
    blocks = [(queries_a, queries_b, offset + jnp.arange(rows, dtype=jnp.int32), cum_gates)]
    initial = tuple(
        (
            (
                empty_state(block[2].shape[0], heads, width_a),
                empty_state(block[2].shape[0], heads, width_b),
            )
            for block in blocks
        )
    )
    start = jnp.int32(0)
    piece_key_a = lax.all_gather(key_a.reshape(rows, heads, width_a), "sp", axis=0, tiled=True)
    piece_value_a = lax.all_gather(value_a.reshape(rows, heads, width_a), "sp", axis=0, tiled=True)
    piece_key_b = lax.all_gather(key_b.reshape(rows, heads, width_b), "sp", axis=0, tiled=True)
    piece_value_b = lax.all_gather(value_b.reshape(rows, heads, width_b), "sp", axis=0, tiled=True)
    item_count = piece_key_a.shape[0]
    key_pos = jnp.arange(item_count, dtype=jnp.int32)
    updated = []
    for state, (block_a, block_b, position, block_gate) in zip(initial, blocks):

        def compute(current):
            mask = key_pos[None, :] <= position[:, None]
            return (
                update_state(
                    current[0],
                    block_a,
                    piece_key_a,
                    piece_value_a,
                    block_gate[:, 0, :],
                    gates_all[:, 0, :],
                    mask,
                    width_a,
                ),
                update_state(
                    current[1],
                    block_b,
                    piece_key_b,
                    piece_value_b,
                    block_gate[:, 1, :],
                    gates_all[:, 1, :],
                    mask,
                    width_b,
                ),
            )

        updated.append(lax.cond(start <= position[-1], compute, lambda current: current, state))
    folded = tuple(updated)
    attn_a = finish(folded[0][0])
    attn_b = finish(folded[0][1])
    proj = lax.psum_scatter(
        (
            jnp.dot(attn_a, out_a, preferred_element_type=jnp.float32)
            + jnp.dot(attn_b, out_b, preferred_element_type=jnp.float32)
        ).astype(jnp.bfloat16),
        "tp",
        scatter_dimension=0,
        tiled=True,
    )
    post = rms_scale(proj.astype(jnp.float32), post_gain.astype(jnp.float32))
    mid_stream = (residual_in.astype(jnp.float32) + post).astype(jnp.bfloat16)
    normed = rms_scale(mid_stream.astype(jnp.float32), pre_gain.astype(jnp.float32)).astype(
        jnp.bfloat16
    )
    selected_count = expert_ids.shape[1]
    columns = normed.shape[1] // narrow
    slots = rows * selected_count * 5 // (4 * group_size)
    flat_experts = expert_ids.reshape(-1)
    onehot = (flat_experts[:, None] == jnp.arange(group_size, dtype=jnp.int32)[None, :]).astype(
        jnp.int32
    )
    rank = jnp.sum((jnp.cumsum(onehot, axis=0) - onehot) * onehot, axis=1)
    target = flat_experts * slots + rank
    owner = jnp.arange(rows * selected_count, dtype=jnp.int32) // selected_count
    table = jnp.full((group_size * slots,), -1, jnp.int32).at[target].set(owner)
    live = table >= 0
    source = jnp.maximum(table, 0)
    weighting = jnp.sum(
        expert_weights[:, :, None]
        * (
            target.reshape(rows, selected_count)[:, :, None]
            == jnp.arange(group_size * slots, dtype=jnp.int32)[None, None, :]
        ),
        axis=1,
    )
    column_rows = lax.all_to_all(normed, "tp", split_axis=1, concat_axis=0, tiled=True)
    outgoing = jnp.where(live[:, None], column_rows[source], jnp.zeros((), jnp.bfloat16))
    outgoing = outgoing.reshape(group_size, slots, columns)
    arrived = lax.all_to_all(outgoing, "sp", split_axis=0, concat_axis=0, tiled=True)
    flat = arrived.reshape(-1, columns)
    piece = lax.all_gather(flat, "tp", axis=1, tiled=True)
    gate_rows = w_gate[0]
    up_rows = w_up[0]
    gate = jnp.dot(piece, gate_rows, preferred_element_type=jnp.float32)
    upward = jnp.dot(piece, up_rows, preferred_element_type=jnp.float32)
    hidden_rows = (jax.nn.silu(gate) * upward).astype(jnp.bfloat16)
    hidden = hidden_rows.reshape(arrived.shape[0], arrived.shape[1], -1)
    flat_hidden = hidden.reshape(-1, hidden.shape[2])
    down_cols = w_down[0]
    summed = lax.psum_scatter(
        lax.dot_general(
            down_cols, flat_hidden, (((0,), (1,)), ((), ())), preferred_element_type=jnp.float32
        ).astype(jnp.bfloat16),
        "tp",
        scatter_dimension=0,
        tiled=True,
    )
    returned = lax.all_to_all(
        summed.reshape(columns, group_size, slots), "sp", split_axis=1, concat_axis=1, tiled=True
    )
    mixture_cols = jnp.einsum(
        "te,ce->tc",
        weighting,
        returned.reshape(columns, group_size * slots).astype(jnp.float32),
        precision=lax.Precision.HIGHEST,
    )
    mixture = lax.all_to_all(
        mixture_cols.astype(jnp.bfloat16), "tp", split_axis=0, concat_axis=1, tiled=True
    ).astype(mixture_cols.dtype)
    return (mid_stream.astype(jnp.float32) + mixture).astype(jnp.bfloat16)


def solution(mesh):
    placed = (
        P(("sp", "tp"), None),
        P("sp", "tp"),
        P("sp", "tp"),
        P("sp", "tp"),
        P("sp", "tp"),
        P("sp", "tp"),
        P("sp", "tp"),
        P("sp", None, "tp"),
        P("tp", None),
        P("tp", None),
        P(),
        P(),
        P("sp", None),
        P("sp", None),
        P("sp", None, "tp"),
        P("sp", None, "tp"),
        P("sp", "tp", None),
    )
    return jax.shard_map(
        per_device, mesh=mesh, in_specs=placed, out_specs=P(("sp", "tp"), None), check_vma=False
    )
```

profile of v0, /device:TPU:0, one launch (start us, length us, event | category | flops | bytes accessed | tf_op | source)
XLA Modules:
  0.0 352.2 jit_solution(581141033529459929)
XLA Ops:
  6.5 1.8 copy.59
  8.3 0.0 all-gather.6.cloned.1.call-update
  8.4 0.0 all-gather.8.cloned.1.call-start
  8.4 1.7 copy.60
  10.1 0.0 all-gather.8.cloned.1.call-update
  10.1 0.0 all-gather.10.cloned.1.call-start
  10.2 1.8 copy.61
  11.9 0.0 all-gather.10.cloned.1.call-update
  12.0 0.0 all-gather.12.cloned.1.call-start
  12.0 1.8 copy.62
  13.8 0.0 all-gather.12.cloned.1.call-update
  13.8 0.0 reduce-scatter.3.cloned.1.call-start
  13.9 0.6 slice.21
  15.0 16.0 %all_gather.19 = f32[2048,2,4]{0,2,1:T(4,128)S(1)} all-gather(f32[256,2,4]{0,2,1:T(4,128)} %param.26), channel_id=1, replica_groups=mesh['sp'=8,'tp'=4] {'sp'}, dimensions={0}, use_global_device_ids=true | all-gather | bytes 73728 | tf_op jit(solution)/shard_map/all_gather | solution.py:71
  31.0 4.8 %all-gather.6.cloned.1.call-done = bf16[2048,4,64]{0,2,1:T(8,128)(2,1)} async-done(((bf16[256,4,64]{0,2,1:T(8,128)(2,1)}), bf16[2048,4,64]{0,2,1:T(8,128)(2,1)}) %all-gather.6.cloned.1.call-update) | async-done | bytes 1048592 | tf_op jit(solution)/shard_map/all_gather | solution.py:85
  35.9 25.3 %all-gather.8.cloned.1.call-done = bf16[2048,4,64]{0,2,1:T(8,128)(2,1)} async-done(((bf16[256,4,64]{0,2,1:T(8,128)(2,1)}), bf16[2048,4,64]{0,2,1:T(8,128)(2,1)}) %all-gather.8.cloned.1.call-update) | async-done | bytes 1048592 | tf_op jit(solution)/shard_map/all_gather | solution.py:86
  61.2 31.0 %all-gather.10.cloned.1.call-done = bf16[2048,4,128]{0,2,1:T(8,128)(2,1)} async-done(((bf16[256,4,128]{0,2,1:T(8,128)(2,1)}), bf16[2048,4,128]{0,2,1:T(8,128)(2,1)}) %all-gather.10.cloned.1.call-update) | async-done | bytes 2097168 | tf_op jit(solution)/shard_map/all_gather | solution.py:87
  92.2 31.1 %all-gather.12.cloned.1.call-done = bf16[2048,4,128]{0,2,1:T(8,128)(2,1)} async-done(((bf16[256,4,128]{0,2,1:T(8,128)(2,1)}), bf16[2048,4,128]{0,2,1:T(8,128)(2,1)}) %all-gather.12.cloned.1.call-update) | async-done | bytes 2097168 | tf_op jit(solution)/shard_map/all_gather | solution.py:88
  123.3 22.6 %conditional.1 = (f32[4,256]{1,0:T(4,128)S(1)}, f32[4,256,64]{1,2,0:T(8,128)S(1)}, f32[4,256]{1,0:T(4,128)S(1)}, f32[4,256,128]{1,2,0:T(8,128)S(1)}) conditional(s32[]{:T(128)} %bitcast.9, () %tuple.13, (s32[2048]{0:T(1024)S(1)}, s32[256]{0:T(256)S(1)}, bf16[256,256]{1,0:T(8,128)(2,1)}, bf16[2048,4,64]{0,2,1:T(8,128)(2,1)}, f32[256,2,4]{0,2,1:T(4,128)}, ...), branch_computations={%region_0.0_spmd, %region_1.6_spmd} | conditional | flops 1682438144 | bytes 83133552 | solution.py:119
  123.3 0.7 slice_bitcast_fusion.3
  124.0 1.0 copy.63
  125.1 0.4 broadcast_compare_fusion
  125.4 2.7 fusion.53
  128.2 4.5 %select_reduce_fusion = (f32[4,256]{1,0:T(4,128)S(1)}, f32[4,256]{1,0:T(4,128)S(1)}, f32[4,256,2048]{2,1,0:T(8,128)S(1)}) fusion(f32[4,2048]{1,0:T(4,128)S(1)} %get-tuple-element.97, f32[4,256]{1,0:T(4,128)S(1)} %get-tuple-element.99, pred[256,2048]{1,0:T(8,128)(4,1)S(1)} %broadcast_compare_fusion, f32[4,2048]{1,0:T(4,128)S(1)} %get-tuple-element.96, ...), kind=kOutput, calls=%fused_computation.3 | convolution fusion | flops 557840384 | bytes 19742720 | tf_op jit(solution)/shard_map/cond/branch_1_fun/rhd,khd->hrk/dot_general | solution.py:24
  132.7 2.8 fusion.6
  135.5 5.9 %fusion.3 = (f32[4,256]{1,0:T(4,128)S(1)}, f32[4,256]{1,0:T(4,128)S(1)}) fusion(f32[4,256,2048]{2,1,0:T(8,128)S(1)} %get-tuple-element.100, f32[4,256]{1,0:T(4,128)S(1)} %get-tuple-element.101, f32[4,2048]{1,0:T(4,128)S(1)} %get-tuple-element.97, f32[4,256]{1,0:T(4,128)S(1)} %get-tuple-element.99, pred[256,2048]{1,0:T(8,128)(4,1)S(1)} %broadcast_compare_fusion, ...), kind=kLoop, calls=%fused_computation.11 | loop fusion | flops 25163776 | bytes 17391616 | tf_op jit(solution)/shard_map/cond/branch_1_fun/reduce_sum | solution.py:30
  141.4 4.3 %fusion.4 = f32[4,256,128]{1,2,0:T(8,128)S(1)} fusion(bf16[2048,4,128]{0,2,1:T(8,128)(2,1)} %get-tuple-element.88, f32[4,256,2048]{2,1,0:T(8,128)S(1)} %get-tuple-element.100, f32[4,256]{1,0:T(4,128)S(1)} %get-tuple-element.101, f32[4,2048]{1,0:T(4,128)S(1)} %get-tuple-element.97, f32[4,256]{1,0:T(4,128)S(1)} %get-tuple-element.99, ...), kind=kOutput, calls=%fused_computation.12 | convolution fusion | flops 549453824 | bytes 11575296 | tf_op jit(solution)/shard_map/cond | solution.py:119
  146.0 1.7 fusion.54
  147.8 1.7 fusion.29
  149.5 0.1 copy.67
  149.7 0.1 eq.42
  149.8 0.1 eq.38
  150.0 1.1 reduce-window.6
  151.1 0.2 slice_reduce_fusion
  151.4 0.1 fusion.43
  151.5 0.1 reduce_sum.60
  151.7 0.1 mul.94
  151.8 2.4 scatter_custom_fusion
  154.3 22.3 %reduce-scatter.3.cloned.1.call-done = bf16[64,2048]{1,0:T(8,128)(2,1)} async-done(((bf16[256,2048]{1,0:T(8,128)(2,1)}), bf16[64,2048]{1,0:T(8,128)(2,1)}) %reduce-scatter.3.cloned.1.call-update) | async-done | bytes 262160 | tf_op jit(solution)/shard_map/reduce_scatter | solution.py:123
  176.6 1.1 fusion.34
  177.8 1.3 fusion.38
  179.0 0.7 copy-done.1
  179.7 0.1 fusion.40
  179.9 0.7 copy.87
  180.6 3.4 all-to-all-start
  184.0 0.0 all-gather.14.cloned.1.call-start
  184.1 0.1 broadcast_in_dim.74
  184.2 5.3 %all-to-all-done = bf16[64,4,512]{2,0,1:T(8,128)(2,1)S(1)} async-done(((bf16[64,4,512]{2,0,1:T(8,128)(2,1)}), bf16[64,4,512]{2,0,1:T(8,128)(2,1)S(1)}, u32[]{:S(2)}, u32[]{:S(2)}) %all-to-all-start) | async-done | bytes 262176 | tf_op jit(solution)/shard_map/all_to_all | solution.py:158
  189.5 2.8 gather_fusion
  192.2 0.2 broadcast_select_fusion
  192.4 22.6 %all_to_all.42 = bf16[8,80,512]{2,1,0:T(8,128)(2,1)} all-to-all(bf16[8,80,512]{2,1,0:T(8,128)(2,1)S(1)} %broadcast_select_fusion), channel_id=1, replica_groups=mesh['sp'=8,'tp'=4] {'sp'}, dimensions={0} | all-to-all | bytes 1310720 | tf_op jit(solution)/shard_map/all_to_all | solution.py:161
  215.0 0.0 all-gather.14.cloned.1.call-update
  215.1 0.0 reduce-scatter.5.cloned.1.call-start
  215.1 37.2 %all-gather.14.cloned.1.call-done = bf16[640,2048]{1,0:T(8,128)(2,1)} async-done(((bf16[640,512]{1,0:T(8,128)(2,1)}), bf16[640,2048]{1,0:T(8,128)(2,1)}) %all-gather.14.cloned.1.call-update) | async-done | bytes 2621456 | tf_op jit(solution)/shard_map/all_gather | solution.py:163
  252.4 7.4 %fusion.19 = f32[640,1024]{1,0:T(8,128)} fusion(bf16[640,2048]{1,0:T(8,128)(2,1)} %all-gather.14.cloned.1.call-done, bf16[1,2048,1024]{2,1,0:T(8,128)(2,1)} %param.34), kind=kOutput, calls=%fused_computation.32 | convolution fusion | flops 2684354560 | bytes 9437184 | tf_op jit(solution)/shard_map/dot_general | solution.py:167
  259.7 12.3 %fusion.26 = bf16[2048,640]{0,1:T(8,128)(2,1)} fusion(bf16[1,1024,2048]{2,1,0:T(8,128)(2,1)} %param.35, f32[640,1024]{1,0:T(8,128)} %fusion.19, bf16[640,2048]{1,0:T(8,128)(2,1)} %all-gather.14.cloned.1.call-done, bf16[1,2048,1024]{2,1,0:T(8,128)(2,1)} %param.33), kind=kOutput, calls=%fused_computation.37 | convolution fusion | flops 5373952000 | bytes 16252928 | tf_op jit(solution)/shard_map/dot_general | solution.py:173
  272.0 39.7 %reduce-scatter.5.cloned.1.call-done = bf16[512,640]{0,1:T(8,128)(2,1)} async-done(((bf16[2048,640]{0,1:T(8,128)(2,1)}), bf16[512,640]{0,1:T(8,128)(2,1)}) %reduce-scatter.5.cloned.1.call-update) | async-done | bytes 655376 | tf_op jit(solution)/shard_map/reduce_scatter | solution.py:172
  311.8 4.6 %all-to-all-start.2 = ((bf16[512,8,80]{0,2,1:T(8,128)(2,1)}), bf16[512,8,80]{0,2,1:T(8,128)(2,1)S(1)}, u32[]{:S(2)}, u32[]{:S(2)}) async-start(bf16[512,8,80]{0,2,1:T(8,128)(2,1)} %bitcast.106), calls=%async_computation.4 | async-start | bytes 1310720 | tf_op jit(solution)/shard_map/all_to_all | solution.py:180
  316.3 0.1 copy.70
  316.4 0.2 select_reduce_fusion.2
  316.7 17.8 %all-to-all-done.2 = bf16[512,8,80]{0,2,1:T(8,128)(2,1)S(1)} async-done(((bf16[512,8,80]{0,2,1:T(8,128)(2,1)}), bf16[512,8,80]{0,2,1:T(8,128)(2,1)S(1)}, u32[]{:S(2)}, u32[]{:S(2)}) %all-to-all-start.2) | async-done | bytes 655392 | tf_op jit(solution)/shard_map/all_to_all | solution.py:180
  334.5 0.8 convolution_convert_fusion
  335.3 8.3 %all_to_all.43 = bf16[4,64,512]{2,1,0:T(8,128)(2,1)S(1)} all-to-all(bf16[4,64,512]{2,1,0:T(8,128)(2,1)S(1)} %bitcast.104), channel_id=1, replica_groups=mesh['sp'=8,'tp'=4] {'tp'}, dimensions={0} | all-to-all | bytes 524288 | tf_op jit(solution)/shard_map/all_to_all | solution.py:189
  343.7 1.7 fusion.41
  (43 shorter events, 0.4 us)
Async XLA Ops:
  6.5 141.2 %copy-start = (bf16[512,2048]{1,0:T(8,128)(2,1)S(1)}, bf16[512,2048]{1,0:T(8,128)(2,1)}, u32[]{:S(2)}) copy-start(bf16[512,2048]{1,0:T(8,128)(2,1)} %param.28) | copy-start | bytes 6291460
  6.5 29.3 %all-gather.6.cloned.1.call-start = ((), (), s32[]{:S(2)}) async-start(), calls=%async_computation.6 | async-start | bytes 1179648 | tf_op jit(solution)/shard_map/all_gather | solution.py:85
  8.4 52.8 %all-gather.8.cloned.1.call-start = ((), (), s32[]{:S(2)}) async-start(), calls=%async_computation.7 | async-start | bytes 1179648 | tf_op jit(solution)/shard_map/all_gather | solution.py:86
  10.1 82.1 %all-gather.10.cloned.1.call-start = ((), (), s32[]{:S(2)}) async-start(), calls=%async_computation.8 | async-start | bytes 2359296 | tf_op jit(solution)/shard_map/all_gather | solution.py:87
  12.0 111.3 %all-gather.12.cloned.1.call-start = ((), (), s32[]{:S(2)}) async-start(), calls=%async_computation.9 | async-start | bytes 2359296 | tf_op jit(solution)/shard_map/all_gather | solution.py:88
  13.8 162.8 %reduce-scatter.3.cloned.1.call-start = ((), (), s32[]{:S(2)}) async-start(), calls=%async_computation.10 | async-start | bytes 1310720 | tf_op jit(solution)/shard_map/reduce_scatter | solution.py:123
  124.0 4.1 %copy-start.9 = (bf16[256,512]{1,0:T(8,128)(2,1)S(1)}, bf16[256,512]{1,0:T(8,128)(2,1)}, u32[]{:S(2)}) copy-start(bf16[256,512]{1,0:T(8,128)(2,1)} %get-tuple-element.48) | copy-start | bytes 786436 | tf_op jit(solution)/shard_map/cond
  125.1 3.1 copy-start.7
  128.2 4.5 %copy-start.8 = (bf16[2048,4,64]{0,2,1:T(8,128)(2,1)S(1)}, bf16[2048,4,64]{0,2,1:T(8,128)(2,1)}, u32[]{:S(2)}) copy-start(bf16[2048,4,64]{0,2,1:T(8,128)(2,1)} %get-tuple-element.33) | copy-start | bytes 3145732 | tf_op jit(solution)/shard_map/cond
  145.9 3.6 %copy-start.5 = (s32[256,2]{0,1:T(2,128)S(1)}, s32[256,2]{0,1:T(2,128)}, u32[]{:S(2)}) copy-start(s32[256,2]{0,1:T(2,128)} %param.31) | copy-start | bytes 6148
  146.0 4.0 %copy-start.3 = (bf16[2048]{0:T(1024)(128)(2,1)S(1)}, bf16[2048]{0:T(1024)(128)(2,1)}, u32[]{:S(2)}) copy-start(bf16[2048]{0:T(1024)(128)(2,1)} %param.29) | copy-start | bytes 12292
  146.0 4.0 %copy-start.4 = (bf16[2048]{0:T(1024)(128)(2,1)S(1)}, bf16[2048]{0:T(1024)(128)(2,1)}, u32[]{:S(2)}) copy-start(bf16[2048]{0:T(1024)(128)(2,1)} %param.30) | copy-start | bytes 12292
  146.0 31.7 %copy-start.2 = (bf16[64,2048]{1,0:T(8,128)(2,1)S(1)}, bf16[64,2048]{1,0:T(8,128)(2,1)}, u32[]{:S(2)}) copy-start(bf16[64,2048]{1,0:T(8,128)(2,1)} %param.19) | copy-start | bytes 786436
  179.0 0.7 copy-start.1
  180.6 8.9 %all-to-all-start = ((bf16[64,4,512]{2,0,1:T(8,128)(2,1)}), bf16[64,4,512]{2,0,1:T(8,128)(2,1)S(1)}, u32[]{:S(2)}, u32[]{:S(2)}) async-start(bf16[64,4,512]{2,0,1:T(8,128)(2,1)} %bitcast.94), calls=%async_computation.1 | async-start | bytes 524288 | tf_op jit(solution)/shard_map/all_to_all | solution.py:158
  184.0 68.3 %all-gather.14.cloned.1.call-start = ((), (), s32[]{:S(2)}) async-start(), calls=%async_computation.11 | async-start | bytes 3276800 | tf_op jit(solution)/shard_map/all_gather | solution.py:163
  215.1 96.7 %reduce-scatter.5.cloned.1.call-start = ((), (), s32[]{:S(2)}) async-start(), calls=%async_computation.12 | async-start | bytes 3276800 | tf_op jit(solution)/shard_map/reduce_scatter | solution.py:172
  259.7 56.7 %copy-start.6 = (f32[256,2]{0,1:T(2,128)S(1)}, f32[256,2]{0,1:T(2,128)}, u32[]{:S(2)}) copy-start(f32[256,2]{0,1:T(2,128)} %param.32) | copy-start | bytes 6148
  311.8 22.7 %all-to-all-start.2 = ((bf16[512,8,80]{0,2,1:T(8,128)(2,1)}), bf16[512,8,80]{0,2,1:T(8,128)(2,1)S(1)}, u32[]{:S(2)}, u32[]{:S(2)}) async-start(bf16[512,8,80]{0,2,1:T(8,128)(2,1)} %bitcast.106), calls=%async_computation.4 | async-start | bytes 1310720 | tf_op jit(solution)/shard_map/all_to_all | solution.py:180
Sparse Core Ops, SparseCore 0:
  8.9 26.9 all-gather.5
  37.5 23.6 all-gather.7
  62.8 29.3 all-gather.9
  93.6 29.6 all-gather.11
  149.6 26.9 reduce-scatter.2
  215.2 37.1 all-gather.13
  272.2 39.5 reduce-scatter.4
where the time goes:
time: 353 us; the launch traced here: 352 us
  waiting for transfers between devices  215 us (61%)
  blocking collectives  46.9 us (13%)
  matrix products  38.2 us (11%)
  local copies, waits for them, and re-layouts  17.2 us (5%)
  between operations  14.4 us (4%)
  other arithmetic  12.3 us (3%)
  starting transfers between devices  8.24 us (2%)
    reduce_scatter x1, waiting for transfers between devices, per_device(): lax.psum_scatter(lax.dot_general(down_cols, flat_hidden, (((0,), (1,)), (...  39.7 us
    all_gather x1, waiting for transfers between devices, per_device(): piece = lax.all_gather(flat, 'tp', axis=1, tiled=True)  37.2 us
    all_gather x1, waiting for transfers between devices, per_device(): lax.all_gather(value_b.reshape(rows, heads, width_b), 'sp', axis=0, tiled...  31.1 us
    all_gather x1, waiting for transfers between devices, per_device(): lax.all_gather(key_b.reshape(rows, heads, width_b), 'sp', axis=0, tiled=T...  31 us
    all_gather x1, waiting for transfers between devices, per_device(): lax.all_gather(value_a.reshape(rows, heads, width_a), 'sp', axis=0, tiled...  25.3 us
    all_to_all x1, blocking collectives, per_device(): lax.all_to_all(outgoing, 'sp', split_axis=0, concat_axis=0, tiled=True)  22.6 us
    reduce_scatter x1, waiting for transfers between devices, per_device(): lax.psum_scatter((jnp.dot(attn_a, out_a, preferred_element_type=jnp.float...  22.3 us
    all_to_all x1, waiting for transfers between devices, per_device(): lax.all_to_all(summed.reshape(columns, group_size, slots), 'sp', split_ax...  17.8 us
  transfers between devices with their start and end apart: 9, of which 9 were waited for; matrix products, arithmetic and copies ran while one was open for 3% of the time, Pallas kernels for 0%

commit v1 on v0

--- a/solution.py
+++ b/solution.py
@@ -160,7 +160,7 @@
     outgoing = outgoing.reshape(group_size, slots, columns)
     arrived = lax.all_to_all(outgoing, "sp", split_axis=0, concat_axis=0, tiled=True)
     flat = arrived.reshape(-1, columns)
-    piece = lax.all_gather(flat, "tp", axis=1, tiled=True)
+    piece = jnp.concatenate(lax.all_gather(flat, "tp"), axis=1)
     gate_rows = w_gate[0]
     up_rows = w_up[0]
     gate = jnp.dot(piece, gate_rows, preferred_element_type=jnp.float32)

time: 353 us -> 351 us (level)
  matrix products: 38.2 us -> 31.8 us
  local copies, waits for them, and re-layouts: 17.2 us -> 21.6 us
    dot_general x1, matrix products: 12.3 us -> 4.18 us  [per_device(): lax.dot_general(down_cols, flat_hidden, (((0,), (1,)), ((), ())), preferr...]
    all_gather x0 -> x1, local copies, waits for them, and re-layouts: none -> 4.38 us  [per_device(): piece = jnp.concatenate(lax.all_gather(flat, 'tp'), axis=1)]
    unnamed x19 -> x25, local copies, waits for them, and re-layouts: 7.91 us -> 7.93 us
where the time goes in v1:
time: 351 us; the launch traced here: 350 us
  waiting for transfers between devices  215 us (61%)
  blocking collectives  46.9 us (13%)
  matrix products  31.8 us (9%)
  local copies, waits for them, and re-layouts  21.6 us (6%)
  between operations  14.5 us (4%)
  other arithmetic  12.3 us (4%)
  starting transfers between devices  8.27 us (2%)
    reduce_scatter x1, waiting for transfers between devices, per_device(): lax.psum_scatter(lax.dot_general(down_cols, flat_hidden, (((0,), (1,)), (...  39.7 us
    all_gather x1, waiting for transfers between devices, per_device(): piece = jnp.concatenate(lax.all_gather(flat, 'tp'), axis=1)  37.4 us
    all_gather x1, waiting for transfers between devices, per_device(): lax.all_gather(value_b.reshape(rows, heads, width_b), 'sp', axis=0, tiled...  31.1 us
    all_gather x1, waiting for transfers between devices, per_device(): lax.all_gather(key_b.reshape(rows, heads, width_b), 'sp', axis=0, tiled=T...  31 us
    all_gather x1, waiting for transfers between devices, per_device(): lax.all_gather(value_a.reshape(rows, heads, width_a), 'sp', axis=0, tiled...  25.1 us
    all_to_all x1, blocking collectives, per_device(): lax.all_to_all(outgoing, 'sp', split_axis=0, concat_axis=0, tiled=True)  22.7 us
    reduce_scatter x1, waiting for transfers between devices, per_device(): lax.psum_scatter((jnp.dot(attn_a, out_a, preferred_element_type=jnp.float...  22.3 us
    all_to_all x1, waiting for transfers between devices, per_device(): lax.all_to_all(summed.reshape(columns, group_size, slots), 'sp', split_ax...  17.8 us
  transfers between devices with their start and end apart: 9, of which 9 were waited for; matrix products, arithmetic and copies ran while one was open for 3% of the time, Pallas kernels for 0%

profile of v1, /device:TPU:0, one launch (start us, length us, event | category | flops | bytes accessed | tf_op | source)
XLA Modules:
  0.0 350.4 jit_solution(4038256579388415200)
XLA Ops:
  6.5 1.8 copy.77
  8.4 0.0 all-gather.8.cloned.1.call-start
  8.4 1.7 copy.78
  10.1 0.0 all-gather.10.cloned.1.call-start
  10.2 1.8 copy.79
  12.0 0.0 all-gather.10.cloned.1.call-update
  12.0 0.0 all-gather.12.cloned.1.call-start
  12.0 1.8 copy.80
  13.8 0.0 all-gather.12.cloned.1.call-update
  13.8 0.0 reduce-scatter.3.cloned.1.call-start
  13.9 0.6 slice.21
  15.2 16.0 %all_gather.19 = f32[2048,2,4]{0,2,1:T(4,128)S(1)} all-gather(f32[256,2,4]{0,2,1:T(4,128)} %param.26), channel_id=1, replica_groups=mesh['sp'=8,'tp'=4] {'sp'}, dimensions={0}, use_global_device_ids=true | all-gather | bytes 73728 | tf_op jit(solution)/shard_map/all_gather | solution.py:71
  31.1 4.8 %all-gather.6.cloned.1.call-done = bf16[2048,4,64]{0,2,1:T(8,128)(2,1)} async-done(((bf16[256,4,64]{0,2,1:T(8,128)(2,1)}), bf16[2048,4,64]{0,2,1:T(8,128)(2,1)}) %all-gather.6.cloned.1.call-update) | async-done | bytes 1048592 | tf_op jit(solution)/shard_map/all_gather | solution.py:85
  36.0 25.1 %all-gather.8.cloned.1.call-done = bf16[2048,4,64]{0,2,1:T(8,128)(2,1)} async-done(((bf16[256,4,64]{0,2,1:T(8,128)(2,1)}), bf16[2048,4,64]{0,2,1:T(8,128)(2,1)}) %all-gather.8.cloned.1.call-update) | async-done | bytes 1048592 | tf_op jit(solution)/shard_map/all_gather | solution.py:86
  61.1 31.0 %all-gather.10.cloned.1.call-done = bf16[2048,4,128]{0,2,1:T(8,128)(2,1)} async-done(((bf16[256,4,128]{0,2,1:T(8,128)(2,1)}), bf16[2048,4,128]{0,2,1:T(8,128)(2,1)}) %all-gather.10.cloned.1.call-update) | async-done | bytes 2097168 | tf_op jit(solution)/shard_map/all_gather | solution.py:87
  92.1 31.1 %all-gather.12.cloned.1.call-done = bf16[2048,4,128]{0,2,1:T(8,128)(2,1)} async-done(((bf16[256,4,128]{0,2,1:T(8,128)(2,1)}), bf16[2048,4,128]{0,2,1:T(8,128)(2,1)}) %all-gather.12.cloned.1.call-update) | async-done | bytes 2097168 | tf_op jit(solution)/shard_map/all_gather | solution.py:88
  123.2 22.6 %conditional.1 = (f32[4,256]{1,0:T(4,128)S(1)}, f32[4,256,64]{1,2,0:T(8,128)S(1)}, f32[4,256]{1,0:T(4,128)S(1)}, f32[4,256,128]{1,2,0:T(8,128)S(1)}) conditional(s32[]{:T(128)} %bitcast.9, () %tuple.13, (s32[2048]{0:T(1024)S(1)}, s32[256]{0:T(256)S(1)}, bf16[256,256]{1,0:T(8,128)(2,1)}, bf16[2048,4,64]{0,2,1:T(8,128)(2,1)}, f32[256,2,4]{0,2,1:T(4,128)}, ...), branch_computations={%region_0.0_spmd, %region_1.6_spmd} | conditional | flops 1682438144 | bytes 83133552 | solution.py:119
  123.2 0.7 slice_bitcast_fusion.3
  123.9 1.0 copy.81
  125.0 0.4 broadcast_compare_fusion
  125.4 2.7 fusion.50
  128.1 4.5 %select_reduce_fusion = (f32[4,256]{1,0:T(4,128)S(1)}, f32[4,256]{1,0:T(4,128)S(1)}, f32[4,256,2048]{2,1,0:T(8,128)S(1)}) fusion(f32[4,2048]{1,0:T(4,128)S(1)} %get-tuple-element.107, f32[4,256]{1,0:T(4,128)S(1)} %get-tuple-element.109, pred[256,2048]{1,0:T(8,128)(4,1)S(1)} %broadcast_compare_fusion, f32[4,2048]{1,0:T(4,128)S(1)} %get-tuple-element.106, ...), kind=kOutput, calls=%fused_computation.3 | convolution fusion | flops 557840384 | bytes 19742720 | tf_op jit(solution)/shard_map/cond/branch_1_fun/rhd,khd->hrk/dot_general | solution.py:24
  132.6 2.8 fusion.6
  135.4 5.9 %fusion.3 = (f32[4,256]{1,0:T(4,128)S(1)}, f32[4,256]{1,0:T(4,128)S(1)}) fusion(f32[4,256,2048]{2,1,0:T(8,128)S(1)} %get-tuple-element.110, f32[4,256]{1,0:T(4,128)S(1)} %get-tuple-element.111, f32[4,2048]{1,0:T(4,128)S(1)} %get-tuple-element.107, f32[4,256]{1,0:T(4,128)S(1)} %get-tuple-element.109, pred[256,2048]{1,0:T(8,128)(4,1)S(1)} %broadcast_compare_fusion, ...), kind=kLoop, calls=%fused_computation.11 | loop fusion | flops 25163776 | bytes 17391616 | tf_op jit(solution)/shard_map/cond/branch_1_fun/reduce_sum | solution.py:30
  141.3 4.3 %fusion.4 = f32[4,256,128]{1,2,0:T(8,128)S(1)} fusion(bf16[2048,4,128]{0,2,1:T(8,128)(2,1)} %get-tuple-element.98, f32[4,256,2048]{2,1,0:T(8,128)S(1)} %get-tuple-element.110, f32[4,256]{1,0:T(4,128)S(1)} %get-tuple-element.111, f32[4,2048]{1,0:T(4,128)S(1)} %get-tuple-element.107, f32[4,256]{1,0:T(4,128)S(1)} %get-tuple-element.109, ...), kind=kOutput, calls=%fused_computation.12 | convolution fusion | flops 549453824 | bytes 11575296 | tf_op jit(solution)/shard_map/cond | solution.py:119
  145.9 1.7 fusion.51
  147.7 1.7 fusion.29
  149.4 0.1 copy.85
  149.6 0.1 eq.42
  149.7 0.1 eq.38
  149.9 1.1 reduce-window.6
  151.1 0.2 slice_reduce_fusion
  151.3 0.1 fusion.41
  151.4 0.1 reduce_sum.60
  151.6 0.1 mul.94
  151.8 2.4 scatter_custom_fusion
  154.2 22.3 %reduce-scatter.3.cloned.1.call-done = bf16[64,2048]{1,0:T(8,128)(2,1)} async-done(((bf16[256,2048]{1,0:T(8,128)(2,1)}), bf16[64,2048]{1,0:T(8,128)(2,1)}) %reduce-scatter.3.cloned.1.call-update) | async-done | bytes 262160 | tf_op jit(solution)/shard_map/reduce_scatter | solution.py:123
  176.6 1.1 fusion.32
  177.7 1.3 fusion.36
  179.0 0.7 copy-done.2
  179.7 0.1 fusion.38
  179.8 0.7 copy.106
  180.5 3.4 all-to-all-start
  183.9 0.0 all-gather.14.cloned.1.call-start
  184.0 0.1 broadcast_in_dim.74
  184.1 5.3 %all-to-all-done = bf16[64,4,512]{2,0,1:T(8,128)(2,1)S(1)} async-done(((bf16[64,4,512]{2,0,1:T(8,128)(2,1)}), bf16[64,4,512]{2,0,1:T(8,128)(2,1)S(1)}, u32[]{:S(2)}, u32[]{:S(2)}) %all-to-all-start) | async-done | bytes 262176 | tf_op jit(solution)/shard_map/all_to_all | solution.py:158
  189.4 2.8 gather_fusion
  192.2 0.2 broadcast_select_fusion
  192.3 22.7 %all_to_all.42 = bf16[8,80,512]{2,1,0:T(8,128)(2,1)} all-to-all(bf16[8,80,512]{2,1,0:T(8,128)(2,1)S(1)} %broadcast_select_fusion), channel_id=1, replica_groups=mesh['sp'=8,'tp'=4] {'sp'}, dimensions={0} | all-to-all | bytes 1310720 | tf_op jit(solution)/shard_map/all_to_all | solution.py:161
  215.0 0.0 all-gather.14.cloned.1.call-update
  215.0 0.0 reduce-scatter.5.cloned.1.call-start
  215.0 37.4 %all-gather.14.cloned.1.call-done = bf16[4,640,512]{2,1,0:T(8,128)(2,1)} async-done(((bf16[1,640,512]{2,1,0:T(8,128)(2,1)}), bf16[4,640,512]{2,1,0:T(8,128)(2,1)}) %all-gather.14.cloned.1.call-update) | async-done | bytes 2621456 | tf_op jit(solution)/shard_map/all_gather | solution.py:163
  252.4 4.4 %copy.90 = bf16[4,640,512]{1,2,0:T(8,128)(2,1)} copy(bf16[4,640,512]{2,1,0:T(8,128)(2,1)} %all-gather.14.cloned.1.call-done) | data formatting | bytes 5242880 | tf_op jit(solution)/shard_map/all_gather | solution.py:163
  256.8 5.6 %fusion.19 = f32[640,1024]{1,0:T(8,128)S(1)} fusion(bf16[640,2048]{0,1:T(8,128)(2,1)} %bitcast.99, bf16[1,2048,1024]{2,1,0:T(8,128)(2,1)} %param.34), kind=kOutput, calls=%fused_computation.32 | convolution fusion | flops 2684354560 | bytes 9437184 | tf_op jit(solution)/shard_map/dot_general | solution.py:167
  262.5 3.5 multiply_convert_fusion
  266.0 4.2 %fusion.26 = bf16[2048,640]{0,1:T(8,128)(2,1)} fusion(bf16[640,1024]{1,0:T(8,128)(2,1)S(1)} %multiply_convert_fusion, bf16[1,1024,2048]{2,1,0:T(8,128)(2,1)S(1)} %copy-done.9), kind=kOutput, calls=%fused_computation.37 | convolution fusion | flops 2685665280 | bytes 8126464 | tf_op jit(solution)/shard_map/dot_general | solution.py:173
  270.2 39.7 %reduce-scatter.5.cloned.1.call-done = bf16[512,640]{0,1:T(8,128)(2,1)} async-done(((bf16[2048,640]{0,1:T(8,128)(2,1)}), bf16[512,640]{0,1:T(8,128)(2,1)}) %reduce-scatter.5.cloned.1.call-update) | async-done | bytes 655376 | tf_op jit(solution)/shard_map/reduce_scatter | solution.py:172
  309.9 4.6 %all-to-all-start.2 = ((bf16[512,8,80]{0,2,1:T(8,128)(2,1)}), bf16[512,8,80]{0,2,1:T(8,128)(2,1)S(1)}, u32[]{:S(2)}, u32[]{:S(2)}) async-start(bf16[512,8,80]{0,2,1:T(8,128)(2,1)} %bitcast.110), calls=%async_computation.4 | async-start | bytes 1310720 | tf_op jit(solution)/shard_map/all_to_all | solution.py:180
  314.5 0.1 copy.88
  314.6 0.2 select_reduce_fusion.2
  314.8 17.8 %all-to-all-done.2 = bf16[512,8,80]{0,2,1:T(8,128)(2,1)S(1)} async-done(((bf16[512,8,80]{0,2,1:T(8,128)(2,1)}), bf16[512,8,80]{0,2,1:T(8,128)(2,1)S(1)}, u32[]{:S(2)}, u32[]{:S(2)}) %all-to-all-start.2) | async-done | bytes 655392 | tf_op jit(solution)/shard_map/all_to_all | solution.py:180
  332.7 0.8 convolution_convert_fusion
  333.5 8.3 %all_to_all.43 = bf16[4,64,512]{2,1,0:T(8,128)(2,1)S(1)} all-to-all(bf16[4,64,512]{2,1,0:T(8,128)(2,1)S(1)} %bitcast.108), channel_id=1, replica_groups=mesh['sp'=8,'tp'=4] {'tp'}, dimensions={0} | all-to-all | bytes 524288 | tf_op jit(solution)/shard_map/all_to_all | solution.py:189
  341.8 1.7 fusion.39
  (51 shorter events, 0.4 us)
Async XLA Ops:
  6.5 141.1 %copy-start = (bf16[512,2048]{1,0:T(8,128)(2,1)S(1)}, bf16[512,2048]{1,0:T(8,128)(2,1)}, u32[]{:S(2)}) copy-start(bf16[512,2048]{1,0:T(8,128)(2,1)} %param.28) | copy-start | bytes 6291460
  6.5 29.4 %all-gather.6.cloned.1.call-start = ((), (), s32[]{:S(2)}) async-start(), calls=%async_computation.6 | async-start | bytes 1179648 | tf_op jit(solution)/shard_map/all_gather | solution.py:85
  8.4 52.8 %all-gather.8.cloned.1.call-start = ((), (), s32[]{:S(2)}) async-start(), calls=%async_computation.7 | async-start | bytes 1179648 | tf_op jit(solution)/shard_map/all_gather | solution.py:86
  10.1 82.0 %all-gather.10.cloned.1.call-start = ((), (), s32[]{:S(2)}) async-start(), calls=%async_computation.8 | async-start | bytes 2359296 | tf_op jit(solution)/shard_map/all_gather | solution.py:87
  12.0 111.2 %all-gather.12.cloned.1.call-start = ((), (), s32[]{:S(2)}) async-start(), calls=%async_computation.9 | async-start | bytes 2359296 | tf_op jit(solution)/shard_map/all_gather | solution.py:88
  13.8 162.7 %reduce-scatter.3.cloned.1.call-start = ((), (), s32[]{:S(2)}) async-start(), calls=%async_computation.10 | async-start | bytes 1310720 | tf_op jit(solution)/shard_map/reduce_scatter | solution.py:123
  123.9 4.1 %copy-start.12 = (bf16[256,512]{1,0:T(8,128)(2,1)S(1)}, bf16[256,512]{1,0:T(8,128)(2,1)}, u32[]{:S(2)}) copy-start(bf16[256,512]{1,0:T(8,128)(2,1)} %get-tuple-element.48) | copy-start | bytes 786436 | tf_op jit(solution)/shard_map/cond
  125.0 3.1 copy-start.10
  128.1 4.5 %copy-start.11 = (bf16[2048,4,64]{0,2,1:T(8,128)(2,1)S(1)}, bf16[2048,4,64]{0,2,1:T(8,128)(2,1)}, u32[]{:S(2)}) copy-start(bf16[2048,4,64]{0,2,1:T(8,128)(2,1)} %get-tuple-element.33) | copy-start | bytes 3145732 | tf_op jit(solution)/shard_map/cond
  145.8 3.6 %copy-start.6 = (s32[256,2]{0,1:T(2,128)S(1)}, s32[256,2]{0,1:T(2,128)}, u32[]{:S(2)}) copy-start(s32[256,2]{0,1:T(2,128)} %param.31) | copy-start | bytes 6148
  145.9 4.0 %copy-start.4 = (bf16[2048]{0:T(1024)(128)(2,1)S(1)}, bf16[2048]{0:T(1024)(128)(2,1)}, u32[]{:S(2)}) copy-start(bf16[2048]{0:T(1024)(128)(2,1)} %param.29) | copy-start | bytes 12292
  145.9 4.0 %copy-start.5 = (bf16[2048]{0:T(1024)(128)(2,1)S(1)}, bf16[2048]{0:T(1024)(128)(2,1)}, u32[]{:S(2)}) copy-start(bf16[2048]{0:T(1024)(128)(2,1)} %param.30) | copy-start | bytes 12292
  145.9 31.7 %copy-start.3 = (bf16[64,2048]{1,0:T(8,128)(2,1)S(1)}, bf16[64,2048]{1,0:T(8,128)(2,1)}, u32[]{:S(2)}) copy-start(bf16[64,2048]{1,0:T(8,128)(2,1)} %param.19) | copy-start | bytes 786436
  178.9 0.7 copy-start.2
  180.5 8.8 %all-to-all-start = ((bf16[64,4,512]{2,0,1:T(8,128)(2,1)}), bf16[64,4,512]{2,0,1:T(8,128)(2,1)S(1)}, u32[]{:S(2)}, u32[]{:S(2)}) async-start(bf16[64,4,512]{2,0,1:T(8,128)(2,1)} %bitcast.96), calls=%async_computation.1 | async-start | bytes 524288 | tf_op jit(solution)/shard_map/all_to_all | solution.py:158
  183.9 68.5 %all-gather.14.cloned.1.call-start = ((), (), s32[]{:S(2)}) async-start(), calls=%async_computation.11 | async-start | bytes 3276800 | tf_op jit(solution)/shard_map/all_gather | solution.py:163
  215.0 94.9 %reduce-scatter.5.cloned.1.call-start = ((), (), s32[]{:S(2)}) async-start(), calls=%async_computation.12 | async-start | bytes 3276800 | tf_op jit(solution)/shard_map/reduce_scatter | solution.py:172
  256.8 5.7 %copy-start.1 = (bf16[4,640,512]{1,2,0:T(8,128)(2,1)S(1)}, bf16[4,640,512]{1,2,0:T(8,128)(2,1)}, u32[]{:S(2)}) copy-start(bf16[4,640,512]{1,2,0:T(8,128)(2,1)} %copy.90) | copy-start | bytes 7864324
  256.8 5.7 %copy-start.8 = (bf16[1,2048,1024]{2,1,0:T(8,128)(2,1)S(1)}, bf16[1,2048,1024]{2,1,0:T(8,128)(2,1)}, u32[]{:S(2)}) copy-start(bf16[1,2048,1024]{2,1,0:T(8,128)(2,1)} %param.33) | copy-start | bytes 12582916
  262.5 3.5 copy-start.9
  266.0 48.6 %copy-start.7 = (f32[256,2]{0,1:T(2,128)S(1)}, f32[256,2]{0,1:T(2,128)}, u32[]{:S(2)}) copy-start(f32[256,2]{0,1:T(2,128)} %param.32) | copy-start | bytes 6148
  309.9 22.7 %all-to-all-start.2 = ((bf16[512,8,80]{0,2,1:T(8,128)(2,1)}), bf16[512,8,80]{0,2,1:T(8,128)(2,1)S(1)}, u32[]{:S(2)}, u32[]{:S(2)}) async-start(bf16[512,8,80]{0,2,1:T(8,128)(2,1)} %bitcast.110), calls=%async_computation.4 | async-start | bytes 1310720 | tf_op jit(solution)/shard_map/all_to_all | solution.py:180
Sparse Core Ops, SparseCore 0:
  8.9 27.0 all-gather.5
  37.6 23.5 all-gather.7
  62.7 29.3 all-gather.9
  93.6 29.6 all-gather.11
  149.6 26.9 reduce-scatter.2
  215.1 37.2 all-gather.13
  270.3 39.5 reduce-scatter.4
